TPU v7x, 32 devices: a whole 2x2x4 slice. The times are simulated.
32 devices in a mesh: fs: 4 (over y, x), tp: 8 (over z, core).
Axes of the slice: x: 2, y: 2, z: 4, core: 2. Of those that a mesh axis runs over, the one named last changes fastest.
Arguments:
- tokens: bfloat16 [2048, 2048], P('fs', 'tp'), may hold values from -6 to 6
- norm_gain: float32 [2048], P('fs'), may hold values from 0.1 to 1.9
- gate_train: float32 [2048, 8192], P('fs', 'tp'), may hold values from -0.125 to 0.125
- up_train: float32 [2048, 8192], P('fs', 'tp'), may hold values from -0.125 to 0.125
- down_train: float32 [8192, 2048], P('fs', 'tp'), may hold values from -0.0625 to 0.0625
Outputs:
- gate_serve: bfloat16 [2048, 8192], P(None, 'tp')
- up_serve: bfloat16 [2048, 8192], P(None, 'tp')
- down_serve: bfloat16 [8192, 2048], P('tp')
- layer_out: bfloat16 [2048, 2048], P(('fs', 'tp'))
All inputs are finite; a program needn't handle non-finite values.
Results may differ from a plain program's by a relative error of at most 0.024.
Values may be sent and summed in bfloat16 or wider, within the bound.
A program may use at most 64 MiB of HBM per device.

v0:
```python
import jax
import jax.numpy as jnp
from jax import lax
from jax.sharding import PartitionSpec as P

D = 2048
epsilon = 1e-06


def body(tokens, norm_gain, gate_train, up_train, down_train):
    gate_local = (norm_gain[:, None] * gate_train).astype(jnp.bfloat16)
    up_local = (norm_gain[:, None] * up_train).astype(jnp.bfloat16)
    down_local = down_train.astype(jnp.bfloat16)
    features = lax.all_gather(tokens, "tp", axis=1, tiled=True)
    wide = features.astype(jnp.float32)
    squares = jnp.sum(wide * wide, axis=1)
    gate_whole, up_whole = (
        lax.all_gather(gate_local, "fs", axis=0, tiled=True),
        lax.all_gather(up_local, "fs", axis=0, tiled=True),
    )
    gate_sum = jnp.dot(features, gate_whole, preferred_element_type=jnp.float32)
    up_sum = jnp.dot(features, up_whole, preferred_element_type=jnp.float32)
    down_rows = lax.all_gather(down_local, "fs", axis=0, tiled=True)
    down_whole = lax.all_to_all(down_rows, "tp", split_axis=0, concat_axis=1, tiled=True)
    scale = lax.rsqrt(squares / D + epsilon)[:, None]
    hidden = (jax.nn.silu(gate_sum * scale) * (up_sum * scale)).astype(jnp.bfloat16)
    mixed = lax.psum_scatter(
        jnp.dot(hidden, down_whole, preferred_element_type=jnp.float32).astype(jnp.bfloat16),
        "tp",
        scatter_dimension=0,
        tiled=True,
    )
    return (gate_whole, up_whole, down_whole, mixed)


def solution(mesh):
    return jax.shard_map(
        body,
        mesh=mesh,
        in_specs=(P("fs", "tp"), P("fs"), P("fs", "tp"), P("fs", "tp"), P("fs", "tp")),
        out_specs=(P(None, "tp"), P(None, "tp"), P("tp", None), P(("fs", "tp"), None)),
        check_vma=False,
    )
```

profile of v0, /device:TPU:0, one launch (start us, length us, event | category | flops | bytes accessed | tf_op | source)
XLA Modules:
  0.0 293.7 jit_solution(2137613969868247611)
XLA Ops:
  7.2 0.0 copy-start.2
  7.2 0.0 copy-start.3
  7.2 0.0 all-gather.9.cloned.1.call-start
  7.2 2.8 convert_element_type.20
  10.0 0.0 all-gather.9.cloned.1.call-update
  10.1 0.0 all-gather.11.cloned.1.call-start
  10.1 0.7 all-gather.11.cloned.1.call-update
  10.8 0.0 all-gather.5.cloned.1.call-start
  10.9 0.0 copy-done.2
  10.9 0.0 copy-done.3
  10.9 3.2 %multiply_convert_fusion = (bf16[512,1024]{1,0:T(8,128)(2,1)}, bf16[512,1024]{1,0:T(8,128)(2,1)}) fusion(f32[512,1024]{1,0:T(8,128)S(1)} %copy-done.2, f32[512]{0:T(512)S(1)} %copy-done.3, f32[512,1024]{1,0:T(8,128)} %param.7), kind=kLoop, calls=%fused_computation.9 | loop fusion | flops 2097152 | bytes 6293504 | tf_op jit(solution)/shard_map/convert_element_type | solution.py:12
  14.1 0.0 all-gather.5.cloned.1.call-update
  14.1 51.6 %all-gather.9.cloned.1.call-done = bf16[8192,256]{1,0:T(8,128)(2,1)} async-done(((bf16[2048,256]{1,0:T(8,128)(2,1)}), bf16[8192,256]{1,0:T(8,128)(2,1)}) %all-gather.9.cloned.1.call-update) | async-done | bytes 4194320 | tf_op jit(solution)/shard_map/all_gather | solution.py:23
  65.7 4.6 %all-to-all-start = ((bf16[8,1024,256]{2,1,0:T(8,128)(2,1)}), bf16[8,1024,256]{2,1,0:T(8,128)(2,1)}, u32[]{:S(2)}, u32[]{:S(2)}) async-start(bf16[8,1024,256]{2,1,0:T(8,128)(2,1)} %bitcast.32), calls=%async_computation | async-start | bytes 8388608 | tf_op jit(solution)/shard_map/all_to_all | solution.py:24
  70.3 0.0 all-gather.7.cloned.1.call-start
  70.4 0.5 all-gather.7.cloned.1.call-update
  70.9 0.0 reduce-scatter.2.cloned.1.call-start
  71.0 50.9 %all-gather.11.cloned.1.call-done = bf16[512,2048]{1,0:T(8,128)(2,1)} async-done(((bf16[512,256]{1,0:T(8,128)(2,1)}), bf16[512,2048]{1,0:T(8,128)(2,1)}) %all-gather.11.cloned.1.call-update) | async-done | bytes 2097168 | tf_op jit(solution)/shard_map/all_gather | solution.py:14
  121.8 2.2 multiply_reduce_fusion
  124.1 54.8 %all-gather.5.cloned.1.call-done = bf16[2048,1024]{1,0:T(8,128)(2,1)} async-done(((bf16[512,1024]{1,0:T(8,128)(2,1)}), bf16[2048,1024]{1,0:T(8,128)(2,1)}) %all-gather.5.cloned.1.call-update) | async-done | bytes 4194320 | tf_op jit(solution)/shard_map/all_gather | solution.py:18
  178.9 0.0 copy-done.1
  178.9 5.9 %fusion.5 = f32[1024,512]{1,0:T(8,128)} fusion(bf16[2048,1024]{1,0:T(8,128)(2,1)} %all-gather.5.cloned.1.call-done, bf16[512,2048]{1,0:T(8,128)(2,1)S(1)} %copy-done.1), kind=kOutput, calls=%fused_computation.13 | convolution fusion | flops 2147483648 | bytes 8388608 | tf_op jit(solution)/shard_map/dot_general | solution.py:21
  184.8 0.0 all-to-all-done
  184.8 6.5 %copy.10 = bf16[8,1024,256]{1,2,0:T(8,128)(2,1)} copy(bf16[8,1024,256]{2,1,0:T(8,128)(2,1)} %all-to-all-done) | data formatting | bytes 8388608 | tf_op jit(solution)/shard_map/all_to_all | solution.py:24
  191.2 42.5 %all-gather.7.cloned.1.call-done = bf16[2048,1024]{1,0:T(8,128)(2,1)} async-done(((bf16[512,1024]{1,0:T(8,128)(2,1)}), bf16[2048,1024]{1,0:T(8,128)(2,1)}) %all-gather.7.cloned.1.call-update) | async-done | bytes 4194320 | tf_op jit(solution)/shard_map/all_gather | solution.py:19
  233.7 10.3 %convolution_convert_fusion = bf16[512,2048]{1,0:T(8,128)(2,1)} fusion(bf16[1024,2048]{0,1:T(8,128)(2,1)} %bitcast.30, f32[1024,512]{1,0:T(8,128)} %fusion.5, bf16[2048,1024]{1,0:T(8,128)(2,1)} %all-gather.7.cloned.1.call-done, bf16[512,2048]{1,0:T(8,128)(2,1)S(1)} %copy-done.1, f32[512]{0:T(512)S(1)} %add_rsqrt_fusion), kind=kOutput, calls=%fused_computation.1 | convolution fusion | flops 4300210176 | bytes 14682112 | tf_op jit(solution)/shard_map/dot_general | solution.py:28
  244.0 0.0 reduce-scatter.2.cloned.1.call-update
  244.0 6.4 %copy.11 = bf16[1024,2048]{1,0:T(8,128)(2,1)} copy(bf16[1024,2048]{0,1:T(8,128)(2,1)} %bitcast.31) | data formatting | bytes 8388608
  250.5 29.8 %reduce-scatter.2.cloned.1.call-done = bf16[64,2048]{1,0:T(8,128)(2,1)} async-done(((bf16[512,2048]{1,0:T(8,128)(2,1)}), bf16[64,2048]{1,0:T(8,128)(2,1)}) %reduce-scatter.2.cloned.1.call-update) | async-done | bytes 262160 | tf_op jit(solution)/shard_map/reduce_scatter | solution.py:27
  280.3 4.8 %copy.14 = bf16[2048,1024]{1,0:T(8,128)(2,1)} copy(bf16[2048,1024]{1,0:T(8,128)(2,1)} %all-gather.5.cloned.1.call-done) | data formatting | bytes 8388608
  285.1 0.0 copy-done
  285.1 2.0 copy.15
  (3 shorter events, 0.0 us)
Async XLA Ops:
  7.2 3.7 %copy-start.2 = (f32[512,1024]{1,0:T(8,128)S(1)}, f32[512,1024]{1,0:T(8,128)}, u32[]{:S(2)}) copy-start(f32[512,1024]{1,0:T(8,128)} %param.8) | copy-start | bytes 6291460
  7.2 3.7 %copy-start.3 = (f32[512]{0:T(512)S(1)}, f32[512]{0:T(512)}, u32[]{:S(2)}) copy-start(f32[512]{0:T(512)} %param.6) | copy-start | bytes 6148
  7.2 58.6 %all-gather.9.cloned.1.call-start = ((), (), s32[]{:S(2)}) async-start(), calls=%async_computation.4 | async-start | bytes 5242880 | tf_op jit(solution)/shard_map/all_gather | solution.py:23
  10.1 111.8 %all-gather.11.cloned.1.call-start = ((), (), s32[]{:S(2)}) async-start(), calls=%async_computation.5 | async-start | bytes 2359296 | tf_op jit(solution)/shard_map/all_gather | solution.py:14
  10.8 168.1 %all-gather.5.cloned.1.call-start = ((), (), s32[]{:S(2)}) async-start(), calls=%async_computation.2 | async-start | bytes 5242880 | tf_op jit(solution)/shard_map/all_gather | solution.py:18
  65.7 119.0 %all-to-all-start = ((bf16[8,1024,256]{2,1,0:T(8,128)(2,1)}), bf16[8,1024,256]{2,1,0:T(8,128)(2,1)}, u32[]{:S(2)}, u32[]{:S(2)}) async-start(bf16[8,1024,256]{2,1,0:T(8,128)(2,1)} %bitcast.32), calls=%async_computation | async-start | bytes 8388608 | tf_op jit(solution)/shard_map/all_to_all | solution.py:24
  70.3 163.4 %all-gather.7.cloned.1.call-start = ((), (), s32[]{:S(2)}) async-start(), calls=%async_computation.3 | async-start | bytes 5242880 | tf_op jit(solution)/shard_map/all_gather | solution.py:19
  70.9 209.4 %reduce-scatter.2.cloned.1.call-start = ((), (), s32[]{:S(2)}) async-start(), calls=%async_computation.6 | async-start | bytes 2359296 | tf_op jit(solution)/shard_map/reduce_scatter | solution.py:27
  121.8 57.0 %copy-start.1 = (bf16[512,2048]{1,0:T(8,128)(2,1)S(1)}, bf16[512,2048]{1,0:T(8,128)(2,1)}, u32[]{:S(2)}) copy-start(bf16[512,2048]{1,0:T(8,128)(2,1)} %all-gather.11.cloned.1.call-done) | copy-start | bytes 6291460
  280.3 4.8 %copy-start = (bf16[2048,1024]{1,0:T(8,128)(2,1)S(1)}, bf16[2048,1024]{1,0:T(8,128)(2,1)}, u32[]{:S(2)}) copy-start(bf16[2048,1024]{1,0:T(8,128)(2,1)} %all-gather.7.cloned.1.call-done) | copy-start | bytes 12582916
Sparse Core Ops, SparseCore 0:
  10.4 55.2 all-gather.8
  67.3 54.4 all-gather.10
  124.3 54.5 all-gather.4
  181.1 52.5 all-gather.6
  244.2 36.0 reduce-scatter.1
where the time goes:
time: 294 us
  waiting for transfers between devices  231 us (79%)
  local copies, waits for them, and re-layouts  19.8 us (7%)
  matrix products  16.2 us (6%)
  between operations  13.8 us (5%)
  other arithmetic  8.23 us (3%)
  starting transfers between devices  4.8 us (2%)
    all_gather x1, waiting for transfers between devices, body(): lax.all_gather(gate_local, 'fs', axis=0, tiled=True)  54.8 us
    all_gather x1, waiting for transfers between devices, body(): down_rows = lax.all_gather(down_local, 'fs', axis=0, tiled=True)  51.6 us
    all_gather x1, waiting for transfers between devices, body(): features = lax.all_gather(tokens, 'tp', axis=1, tiled=True)  50.9 us
    all_gather x1, waiting for transfers between devices, body(): lax.all_gather(up_local, 'fs', axis=0, tiled=True)  42.5 us
    reduce_scatter x1, waiting for transfers between devices, body(): lax.psum_scatter(jnp.dot(hidden, down_whole, preferred_element_type=jnp.f...  29.8 us
    unnamed x11, local copies, waits for them, and re-layouts  13.3 us
    dot_general x1, matrix products, body(): jnp.dot(hidden, down_whole, preferred_element_type=jnp.float32)  10.3 us
    all_to_all x1, local copies, waits for them, and re-layouts, body(): lax.all_to_all(down_rows, 'tp', split_axis=0, concat_axis=1, tiled=True)  6.48 us
  transfers between devices with their start and end apart: 6, of which 5 were waited for; matrix products, arithmetic and copies ran while one was open for 8% of the time, Pallas kernels for 0%

commit v1 on v0

--- a/solution.py
+++ b/solution.py
@@ -20,7 +20,12 @@
     )
     gate_sum = jnp.dot(features, gate_whole, preferred_element_type=jnp.float32)
     up_sum = jnp.dot(features, up_whole, preferred_element_type=jnp.float32)
-    down_rows = lax.all_gather(down_local, "fs", axis=0, tiled=True)
+    ring = [down_local]
+    for hop in range(3):
+        ring.append(lax.ppermute(ring[-1], "fs", [(dev, (dev + 1) % 4) for dev in range(4)]))
+    down_rows = jnp.roll(
+        jnp.concatenate(ring[::-1], axis=0), (lax.axis_index("fs") + 1) * ring[0].shape[0], axis=0
+    )
     down_whole = lax.all_to_all(down_rows, "tp", split_axis=0, concat_axis=1, tiled=True)
     scale = lax.rsqrt(squares / D + epsilon)[:, None]
     hidden = (jax.nn.silu(gate_sum * scale) * (up_sum * scale)).astype(jnp.bfloat16)

time: 294 us -> 285 us (0.969)
  waiting for transfers between devices: 231 us -> 208 us
  local copies, waits for them, and re-layouts: 19.8 us -> 27.5 us
  starting transfers between devices: 4.8 us -> 10.4 us
    ppermute x0 -> x3, waiting for transfers between devices: none -> 92.5 us  [body(): lax.ppermute(ring[-1], 'fs', [(dev, (dev + 1) % 4) for dev in range(4)])]
    all_to_all x1, waiting for transfers between devices: 0.01 us -> 84.6 us  [body(): lax.all_to_all(down_rows, 'tp', split_axis=0, concat_axis=1, tiled=True)]
    all_gather x1, waiting for transfers between devices: 54.8 us -> 0.02 us  [body(): lax.all_gather(gate_local, 'fs', axis=0, tiled=True)]
    all_gather x1 -> x0, waiting for transfers between devices: 51.6 us -> none  [body(): down_rows = lax.all_gather(down_local, 'fs', axis=0, tiled=True)]
    all_gather x1, waiting for transfers between devices: 50.9 us -> 0.02 us  [body(): features = lax.all_gather(tokens, 'tp', axis=1, tiled=True)]
    all_gather x1, waiting for transfers between devices: 42.5 us -> 0.01 us  [body(): lax.all_gather(up_local, 'fs', axis=0, tiled=True)]
    unnamed x11 -> x17, local copies, waits for them, and re-layouts: 13.3 us -> 18.6 us
    ppermute x0 -> x3, starting transfers between devices: none -> 4.64 us  [body(): lax.ppermute(ring[-1], 'fs', [(dev, (dev + 1) % 4) for dev in range(4)])]
  transfers between devices with their start and end apart: 6 -> 8, of which waited for: 5 -> 5; matrix products, arithmetic and copies ran while one was open for 8% -> 12% of each run, Pallas kernels for 0% -> 0%
where the time goes in v1:
time: 285 us; the launch traced here: 284 us
  waiting for transfers between devices  208 us (73%)
  local copies, waits for them, and re-layouts  27.5 us (10%)
  matrix products  16.9 us (6%)
  between operations  13.9 us (5%)
  starting transfers between devices  10.4 us (4%)
  other arithmetic  7.21 us (3%)
    ppermute x3, waiting for transfers between devices, body(): lax.ppermute(ring[-1], 'fs', [(dev, (dev + 1) % 4) for dev in range(4)])  92.5 us
    all_to_all x1, waiting for transfers between devices, body(): lax.all_to_all(down_rows, 'tp', split_axis=0, concat_axis=1, tiled=True)  84.6 us
    reduce_scatter x1, waiting for transfers between devices, body(): lax.psum_scatter(jnp.dot(hidden, down_whole, preferred_element_type=jnp.f...  29.7 us
    unnamed x17, local copies, waits for them, and re-layouts  18.6 us
    dot_general x1, matrix products, body(): jnp.dot(hidden, down_whole, preferred_element_type=jnp.float32)  10.3 us
    all_to_all x1, local copies, waits for them, and re-layouts, body(): lax.all_to_all(down_rows, 'tp', split_axis=0, concat_axis=1, tiled=True)  6.57 us
    dot_general x1, matrix products, body(): gate_sum = jnp.dot(features, gate_whole, preferred_element_type=jnp.float32)  6.57 us
  transfers between devices with their start and end apart: 8, of which 5 were waited for; matrix products, arithmetic and copies ran while one was open for 12% of the time, Pallas kernels for 0%

profile of v1, /device:TPU:0, one launch (start us, length us, event | category | flops | bytes accessed | tf_op | source)
XLA Modules:
  0.0 283.9 jit_solution(17187609945986158144)
XLA Ops:
  7.2 0.0 all-gather.8.cloned.1.call-start
  7.2 0.7 all-gather.8.cloned.1.call-update
  7.9 0.0 all-gather.4.cloned.1.call-start
  8.0 1.7 convert_element_type.20
  9.7 3.0 %collective-permute-start = (bf16[2048,256]{1,0:T(8,128)(2,1)S(1)}, bf16[2048,256]{1,0:T(8,128)(2,1)S(1)}, u32[]{:S(2)}, u32[]{:S(2)}) collective-permute-start(bf16[2048,256]{1,0:T(8,128)(2,1)S(1)} %convert_element_type.20), channel_id=1, source_target_pairs={{0,8},{8,16},{16,24},{24,0},{1,9},{9,17},{17,25},{25,1},{2,10},{10... | collective-permute-start | bytes 3145736 | tf_op jit(solution)/shard_map/ppermute | solution.py:25
  12.7 24.1 %collective-permute-done = bf16[2048,256]{1,0:T(8,128)(2,1)S(1)} collective-permute-done((bf16[2048,256]{1,0:T(8,128)(2,1)S(1)}, bf16[2048,256]{1,0:T(8,128)(2,1)S(1)}, u32[]{:S(2)}, u32[]{:S(2)}) %collective-permute-start) | collective-permute-done | bytes 1048608 | tf_op jit(solution)/shard_map/ppermute | solution.py:25
  36.8 0.8 collective-permute-start.1
  37.6 3.2 %multiply_convert_fusion = (bf16[512,1024]{1,0:T(8,128)(2,1)}, bf16[512,1024]{1,0:T(8,128)(2,1)}) fusion(f32[512,1024]{1,0:T(8,128)S(1)} %copy-done.3, f32[512]{0:T(512)} %param.6, f32[512,1024]{1,0:T(8,128)} %param.7), kind=kLoop, calls=%fused_computation.9 | loop fusion | flops 2097152 | bytes 6293504 | tf_op jit(solution)/shard_map/convert_element_type | solution.py:12
  40.8 29.7 %collective-permute-done.1 = bf16[2048,256]{1,0:T(8,128)(2,1)} collective-permute-done((bf16[2048,256]{1,0:T(8,128)(2,1)S(1)}, bf16[2048,256]{1,0:T(8,128)(2,1)}, u32[]{:S(2)}, u32[]{:S(2)}) %collective-permute-start.1) | collective-permute-done | bytes 1048608 | tf_op jit(solution)/shard_map/ppermute | solution.py:25
  70.5 0.8 collective-permute-start.2
  71.4 38.7 %collective-permute-done.2 = bf16[2048,256]{1,0:T(8,128)(2,1)} collective-permute-done((bf16[2048,256]{1,0:T(8,128)(2,1)}, bf16[2048,256]{1,0:T(8,128)(2,1)}, u32[]{:S(2)}, u32[]{:S(2)}) %collective-permute-start.2) | collective-permute-done | bytes 1048608 | tf_op jit(solution)/shard_map/ppermute | solution.py:25
  110.0 1.3 constant_dynamic-update-slice_fusion.7
  111.3 1.3 constant_dynamic-update-slice_fusion.6
  112.6 0.1 constant_dynamic-update-slice_fusion.5
  112.7 0.1 constant_dynamic-update-slice_fusion.4
  112.8 1.3 constant_dynamic-update-slice_fusion.3
  114.1 1.3 constant_dynamic-update-slice_fusion.2
  115.4 0.1 constant_dynamic-update-slice_fusion.1
  115.5 0.1 constant_dynamic-update-slice_fusion
  115.6 2.3 constant_dynamic-slice_fusion
  117.9 5.6 %all-to-all-start = ((bf16[8,1024,256]{2,1,0:T(8,128)(2,1)}), bf16[8,1024,256]{2,1,0:T(8,128)(2,1)}, u32[]{:S(2)}, u32[]{:S(2)}) async-start(bf16[8,1024,256]{2,1,0:T(8,128)(2,1)} %bitcast.29), calls=%async_computation | async-start | bytes 8388608 | tf_op jit(solution)/shard_map/all_to_all | solution.py:29
  123.5 0.7 all-gather.6.cloned.1.call-update
  124.2 0.0 reduce-scatter.2.cloned.1.call-start
  124.3 2.1 multiply_reduce_fusion
  126.4 6.6 %fusion.5 = f32[1024,512]{1,0:T(8,128)} fusion(bf16[2048,1024]{1,0:T(8,128)(2,1)} %all-gather.4.cloned.1.call-done, bf16[512,2048]{1,0:T(8,128)(2,1)} %all-gather.8.cloned.1.call-done), kind=kOutput, calls=%fused_computation.22 | convolution fusion | flops 2147483648 | bytes 8388608 | tf_op jit(solution)/shard_map/dot_general | solution.py:21
  132.9 84.6 %all-to-all-done = bf16[8,1024,256]{2,1,0:T(8,128)(2,1)} async-done(((bf16[8,1024,256]{2,1,0:T(8,128)(2,1)}), bf16[8,1024,256]{2,1,0:T(8,128)(2,1)}, u32[]{:S(2)}, u32[]{:S(2)}) %all-to-all-start) | async-done | bytes 4194336 | tf_op jit(solution)/shard_map/all_to_all | solution.py:29
  217.5 6.6 %copy.9 = bf16[1024,8,256]{0,2,1:T(8,128)(2,1)} copy(bf16[1024,8,256]{2,0,1:T(8,128)(2,1)} %bitcast.1) | data formatting | bytes 8388608 | tf_op jit(solution)/shard_map/all_to_all | solution.py:29
  224.1 10.3 %convolution_convert_fusion = bf16[512,2048]{1,0:T(8,128)(2,1)} fusion(bf16[1024,2048]{0,1:T(8,128)(2,1)} %bitcast.30, f32[1024,512]{1,0:T(8,128)} %fusion.5, bf16[2048,1024]{1,0:T(8,128)(2,1)} %all-gather.6.cloned.1.call-done, bf16[512,2048]{1,0:T(8,128)(2,1)S(1)} %copy-done.2, f32[512]{0:T(512)S(1)} %add_rsqrt_fusion), kind=kOutput, calls=%fused_computation.1 | convolution fusion | flops 4300210176 | bytes 14682112 | tf_op jit(solution)/shard_map/dot_general | solution.py:33
  234.5 6.4 %copy.10 = bf16[1024,2048]{1,0:T(8,128)(2,1)} copy(bf16[1024,2048]{0,1:T(8,128)(2,1)} %bitcast.31) | data formatting | bytes 8388608
  240.9 29.7 %reduce-scatter.2.cloned.1.call-done = bf16[64,2048]{1,0:T(8,128)(2,1)} async-done(((bf16[512,2048]{1,0:T(8,128)(2,1)}), bf16[64,2048]{1,0:T(8,128)(2,1)}) %reduce-scatter.2.cloned.1.call-update) | async-done | bytes 262160 | tf_op jit(solution)/shard_map/reduce_scatter | solution.py:32
  270.6 4.8 %copy.20 = bf16[2048,1024]{1,0:T(8,128)(2,1)} copy(bf16[2048,1024]{1,0:T(8,128)(2,1)} %all-gather.4.cloned.1.call-done) | data formatting | bytes 8388608
  275.4 2.0 copy.21
  (15 shorter events, 0.1 us)
Async XLA Ops:
  7.2 30.4 %copy-start.3 = (f32[512,1024]{1,0:T(8,128)S(1)}, f32[512,1024]{1,0:T(8,128)}, u32[]{:S(2)}) copy-start(f32[512,1024]{1,0:T(8,128)} %param.8) | copy-start | bytes 6291460
  7.2 117.1 %all-gather.8.cloned.1.call-start = ((), (), s32[]{:S(2)}) async-start(), calls=%async_computation.4 | async-start | bytes 2359296 | tf_op jit(solution)/shard_map/all_gather | solution.py:14
  7.9 118.5 %all-gather.4.cloned.1.call-start = ((), (), s32[]{:S(2)}) async-start(), calls=%async_computation.2 | async-start | bytes 5242880 | tf_op jit(solution)/shard_map/all_gather | solution.py:18
  9.7 27.1 %collective-permute-start = (bf16[2048,256]{1,0:T(8,128)(2,1)S(1)}, bf16[2048,256]{1,0:T(8,128)(2,1)S(1)}, u32[]{:S(2)}, u32[]{:S(2)}) collective-permute-start(bf16[2048,256]{1,0:T(8,128)(2,1)S(1)} %convert_element_type.20), channel_id=1, source_target_pairs={{0,8},{8,16},{16,24},{24,0},{1,9},{9,17},{17,25},{25,1},{2,10},{10... | collective-permute-start | bytes 3145736 | tf_op jit(solution)/shard_map/ppermute | solution.py:25
  36.8 33.7 %collective-permute-start.1 = (bf16[2048,256]{1,0:T(8,128)(2,1)S(1)}, bf16[2048,256]{1,0:T(8,128)(2,1)}, u32[]{:S(2)}, u32[]{:S(2)}) collective-permute-start(bf16[2048,256]{1,0:T(8,128)(2,1)S(1)} %collective-permute-done), channel_id=1, source_target_pairs={{0,8},{8,16},{16,24},{24,0},{1,9},{9,17},{17,25},{25,1},{2,10},{10... | collective-permute-start | bytes 3145736 | tf_op jit(solution)/shard_map/ppermute | solution.py:25
  40.8 71.9 %copy-start = (f32[2048,256]{1,0:T(8,128)S(1)}, f32[2048,256]{1,0:T(8,128)}, u32[]{:S(2)}) copy-start(f32[2048,256]{1,0:T(8,128)} %param.9) | copy-start | bytes 6291460
  70.5 39.5 %collective-permute-start.2 = (bf16[2048,256]{1,0:T(8,128)(2,1)}, bf16[2048,256]{1,0:T(8,128)(2,1)}, u32[]{:S(2)}, u32[]{:S(2)}) collective-permute-start(bf16[2048,256]{1,0:T(8,128)(2,1)} %collective-permute-done.1), channel_id=1, source_target_pairs={{0,8},{8,16},{16,24},{24,0},{1,9},{9,17},{17,25},{25,1},{2,10},{10... | collective-permute-start | bytes 3145736 | tf_op jit(solution)/shard_map/ppermute | solution.py:25
  117.9 99.6 %all-to-all-start = ((bf16[8,1024,256]{2,1,0:T(8,128)(2,1)}), bf16[8,1024,256]{2,1,0:T(8,128)(2,1)}, u32[]{:S(2)}, u32[]{:S(2)}) async-start(bf16[8,1024,256]{2,1,0:T(8,128)(2,1)} %bitcast.29), calls=%async_computation | async-start | bytes 8388608 | tf_op jit(solution)/shard_map/all_to_all | solution.py:29
  123.5 100.7 %all-gather.6.cloned.1.call-start = ((), (), s32[]{:S(2)}) async-start(), calls=%async_computation.3 | async-start | bytes 5242880 | tf_op jit(solution)/shard_map/all_gather | solution.py:19
  124.2 146.4 %reduce-scatter.2.cloned.1.call-start = ((), (), s32[]{:S(2)}) async-start(), calls=%async_computation.5 | async-start | bytes 2359296 | tf_op jit(solution)/shard_map/reduce_scatter | solution.py:32
  217.5 6.6 %copy-start.2 = (bf16[512,2048]{1,0:T(8,128)(2,1)S(1)}, bf16[512,2048]{1,0:T(8,128)(2,1)}, u32[]{:S(2)}) copy-start(bf16[512,2048]{1,0:T(8,128)(2,1)} %all-gather.8.cloned.1.call-done) | copy-start | bytes 6291460
  270.6 4.8 %copy-start.1 = (bf16[2048,1024]{1,0:T(8,128)(2,1)S(1)}, bf16[2048,1024]{1,0:T(8,128)(2,1)}, u32[]{:S(2)}) copy-start(bf16[2048,1024]{1,0:T(8,128)(2,1)} %all-gather.6.cloned.1.call-done) | copy-start | bytes 12582916
Sparse Core Ops, SparseCore 0:
  9.6 33.3 all-gather.7
  45.4 73.1 all-gather.3
  126.1 55.0 all-gather.5
  234.6 35.9 reduce-scatter.1
